TPU v7x, 256 devices: a 2x2x32 block of a 4x8x32 slice. The times are simulated.
256 devices in a mesh: grp: 4 (over y, x), ep: 64 (over z, core).
Axes of the slice: x: 2, y: 2, z: 32, core: 2. Of those that a mesh axis runs over, the one named last changes fastest.
The devices are a block of a 4x8x32 slice.
Arguments:
- tokens: bfloat16 [32768, 2048], P(('grp', 'ep')), parts along dimension 0, may hold values from -6 to 6
- norm_gain: float32 [2048], replicated, may hold values from 0.1 to 1.9
- expert_ids: int32 [32768, 2], P(('grp', 'ep')), parts along dimension 0, may hold values from 0 to 15, all different within a row; in each aligned block of 128 rows (0 to 127, 128 to 255, ...) at most 32 rows name the same one
- route_weight: float32 [32768, 2], P(('grp', 'ep')), parts along dimension 0, may hold values from 0.1 to 1
- gate_weight: bfloat16 [64, 2048, 512], P('ep'), may hold values from -0.375 to 0.375
- up_weight: bfloat16 [64, 2048, 512], P('ep'), may hold values from -0.375 to 0.375
- down_weight: bfloat16 [64, 512, 2048], P('ep'), may hold values from -0.03125 to 0.03125
Outputs:
- combined: bfloat16 [32768, 2048], P(('grp', 'ep')), parts along dimension 0
There are 4 independent parts, one for each index of `grp`. A program takes and returns all parts, laid end to end along the dimension named above; an argument that names none is the same for every part. Nothing has to cross between parts.
Inputs may be any that keep to these rules, and one draw needn't show every extreme that they name: `expert_ids`: each token names 2 different experts; among the tokens of one device no expert is named more than 32 times, and in every draw some expert is named exactly 32 times by the tokens of some device.
All inputs are finite; a program needn't handle non-finite values.
Results may differ from a plain program's by a relative error of at most 0.0078.
Values may be sent and summed in bfloat16 or wider, within the bound.
A program may use at most 128 MiB of HBM per device.

v0:
```python
import jax
import jax.numpy as jnp
from jax import lax
from jax.sharding import PartitionSpec as P

SPLIT = 4


EPSILON = 1e-05
clamp_limit = 7.0
sigmoid_slope = 1.702


def swapped(array, axis, bit):
    return lax.ppermute(array, axis, [(i, i ^ 1 << bit) for i in range(lax.axis_size(axis))])


def layer_norm(tokens, norm_gain):
    values = tokens.astype(jnp.float32)
    center = values - jnp.mean(values, axis=-1, keepdims=True)
    spread = jnp.mean(center * center, axis=-1, keepdims=True)
    return (center * lax.rsqrt(spread + EPSILON) * norm_gain).astype(jnp.bfloat16)


def expert_rows(block_rows, gate_weight, up_weight, down_weight):
    gate_pre = jnp.einsum(
        "scd,df->scf", block_rows, gate_weight[0], preferred_element_type=jnp.float32
    )
    up_pre = jnp.einsum("scd,df->scf", block_rows, up_weight[0], preferred_element_type=jnp.float32)
    gate_cut = jnp.minimum(gate_pre, clamp_limit)
    up_cut = jnp.clip(up_pre, -clamp_limit, clamp_limit)
    active = ((up_cut + 1.0) * (gate_cut * jax.nn.sigmoid(gate_cut * sigmoid_slope))).astype(
        jnp.bfloat16
    )
    return jnp.einsum("scf,fd->scd", active, down_weight[0], preferred_element_type=jnp.float32)


def body(tokens, norm_gain, expert_ids, route_weight, gate_weight, up_weight, down_weight):
    normed = layer_norm(tokens, norm_gain)
    devices = lax.axis_size("ep")
    experts = devices // SPLIT
    tok_rows = tokens.shape[0]
    top_count = expert_ids.shape[1]
    width = tokens.shape[1]
    capacity = min(tok_rows, 2 * tok_rows * top_count // experts)
    quarter = capacity // SPLIT
    levels = SPLIT.bit_length() - 1
    position = lax.axis_index("ep")
    flat_ids = expert_ids.reshape(-1)
    onehot = (flat_ids[:, None] == jnp.arange(experts, dtype=jnp.int32)[None, :]).astype(jnp.int32)
    earlier = jnp.cumsum(onehot, axis=0) - onehot
    slot_index = jnp.sum(earlier * onehot, axis=1)
    target = flat_ids * capacity + slot_index
    owners = jnp.arange(flat_ids.shape[0], dtype=jnp.int32) // top_count
    slot_token = jnp.full((experts * capacity,), tok_rows, jnp.int32).at[target].set(owners)
    padded = jnp.concatenate([normed, jnp.zeros((1, width), jnp.bfloat16)], axis=0)
    outgoing = jnp.take(padded, slot_token, axis=0).reshape(experts, capacity, width)
    pieces = outgoing.reshape(devices, quarter, width)
    gathered = lax.all_to_all(pieces, "ep", split_axis=0, concat_axis=0, tiled=True)
    for bit_level in range(levels):
        partner = swapped(gathered, "ep", bit_level)
        upper_bit = position >> bit_level & 1
        first_half = jnp.where(upper_bit == 1, partner, gathered)
        second_half = jnp.where(upper_bit == 1, gathered, partner)
        gathered = jnp.concatenate([first_half, second_half], axis=1)
    partial_value = expert_rows(gathered, gate_weight, up_weight, down_weight)
    length = capacity
    for bit_level in reversed(range(levels)):
        length = length // 2
        upper_bit = position >> bit_level & 1
        kept_rows = lax.dynamic_slice_in_dim(partial_value, upper_bit * length, length, 1)
        sent_rows = lax.dynamic_slice_in_dim(partial_value, (1 - upper_bit) * length, length, 1)
        partial_value = kept_rows + swapped(sent_rows.astype(jnp.bfloat16), "ep", bit_level).astype(
            sent_rows.dtype
        )
    finished = partial_value.astype(jnp.bfloat16)
    returned = lax.all_to_all(finished, "ep", split_axis=0, concat_axis=0, tiled=True)
    results = returned.reshape(experts * capacity, width)
    picked = jnp.take(results, target, axis=0).reshape(tok_rows, top_count, width)
    combined = jnp.sum(route_weight[:, :, None] * picked.astype(jnp.float32), axis=1)
    return combined.astype(jnp.bfloat16)


def solution(mesh):
    placed = (
        P(("grp", "ep"), None),
        P(),
        P(("grp", "ep"), None),
        P(("grp", "ep"), None),
        P("ep", None, None),
        P("ep", None, None),
        P("ep", None, None),
    )
    return jax.shard_map(
        body, mesh=mesh, in_specs=placed, out_specs=P(("grp", "ep"), None), check_vma=False
    )
```

profile of v0, /device:TPU:38, one launch (start us, length us, event | category | flops | bytes accessed | tf_op | source)
XLA Modules:
  0.0 716.8 jit_solution(9506049461779293233)
XLA Ops:
  0.0 0.9 copy.16
  0.9 0.1 eq.34
  1.1 0.1 reshape.90
  1.2 0.7 broadcast_multiply_fusion
  1.9 0.6 reduce-window.6
  2.5 0.2 slice_reduce_fusion
  2.7 0.1 copy.21
  2.8 0.1 mul.77
  3.0 0.1 fusion.18
  3.1 1.4 scatter_custom_fusion
  4.5 1.2 convert_reduce_fusion
  5.7 1.3 fusion.13
  7.1 0.1 broadcast_in_dim.36
  7.2 1.4 fusion.15
  8.7 3.3 gather_fusion
  12.0 1.8 bitcast_select_fusion
  13.8 233.2 %all_to_all.10 = bf16[64,8,2048]{2,1,0:T(8,128)(2,1)} all-to-all(bf16[64,8,2048]{2,1,0:T(8,128)(2,1)S(1)} %bitcast_select_fusion), channel_id=1, replica_groups=mesh['grp'=4,'ep'=64] {'ep'}, dimensions={0} | all-to-all | bytes 4194304 | tf_op jit(solution)/shard_map/all_to_all | solution.py:59
  247.0 0.0 collective-permute-start
  247.0 4.5 collective-permute-done
  251.5 2.5 broadcast_select_fusion.3
  254.0 2.5 pad_maximum_fusion.3
  256.5 0.1 copy-done.3
  256.6 0.7 copy-done.4
  257.3 0.0 collective-permute-start.1
  257.3 92.9 %collective-permute-done.1 = bf16[64,16,2048]{2,1,0:T(8,128)(2,1)} collective-permute-done((bf16[64,16,2048]{2,1,0:T(8,128)(2,1)}, bf16[64,16,2048]{2,1,0:T(8,128)(2,1)}, u32[]{:S(2)}, u32[]{:S(2)}) %collective-permute-start.1) | collective-permute-done | bytes 4194336 | tf_op jit(solution)/shard_map/ppermute | solution.py:15
  350.3 5.0 broadcast_select_fusion.1
  355.3 2.0 copy-done.5
  357.2 1.3 copy-done.6
  358.5 6.1 fusion.1
  364.6 16.5 %fusion.2 = f32[64,32,2048]{2,1,0:T(8,128)} fusion(f32[64,32,512]{2,1,0:T(8,128)} %fusion.1, bf16[64,16,2048]{2,1,0:T(8,128)(2,1)} %copy-done.6, bf16[64,16,2048]{2,1,0:T(8,128)(2,1)} %copy-done.5, bf16[1,512,2048]{2,1,0:T(8,128)(2,1)S(1)} %copy-done, bf16[1,2048,512]{2,1,0:T(8,128)(2,1)} %param.11), kind=kOutput, calls=%fused_computation.14 | convolution fusion | flops 8617197568 | bytes 33554432 | tf_op jit(solution)/shard_map/scf,fd->scd/dot_general | solution.py:35
  381.1 6.0 dynamic-slice_convert_fusion
  387.1 0.3 collective-permute-start.2
  387.4 91.8 %collective-permute-done.2 = bf16[64,16,2048]{2,1,0:T(8,128)(2,1)} collective-permute-done((bf16[64,16,2048]{2,1,0:T(8,128)(2,1)}, bf16[64,16,2048]{2,1,0:T(8,128)(2,1)}, u32[]{:S(2)}, u32[]{:S(2)}) %collective-permute-start.2) | collective-permute-done | bytes 4194336 | tf_op jit(solution)/shard_map/ppermute | solution.py:15
  479.1 5.9 convert_add_fusion
  485.1 3.2 copy-done.2
  488.3 0.3 dynamic-slice_convert_fusion.1
  488.6 0.1 collective-permute-start.3
  488.8 4.3 collective-permute-done.3
  493.0 4.9 add_convert_fusion
  498.0 7.5 %all-to-all-start.1 = ((bf16[64,8,2048]{2,1,0:T(8,128)(2,1)}), bf16[64,8,2048]{2,1,0:T(8,128)(2,1)}, u32[]{:S(2)}, u32[]{:S(2)}) async-start(bf16[64,8,2048]{2,1,0:T(8,128)(2,1)} %add_convert_fusion), calls=%async_computation.1 | async-start | bytes 4194304 | tf_op jit(solution)/shard_map/all_to_all | solution.py:77
  505.5 0.1 reduce_sum.41
  505.7 0.1 copy.19
  505.8 0.1 copy.20
  505.9 0.1 copy.15
  506.0 198.6 %all-to-all-done.1 = bf16[64,8,2048]{2,1,0:T(8,128)(2,1)} async-done(((bf16[64,8,2048]{2,1,0:T(8,128)(2,1)}), bf16[64,8,2048]{2,1,0:T(8,128)(2,1)}, u32[]{:S(2)}, u32[]{:S(2)}) %all-to-all-start.1) | async-done | bytes 2097184 | tf_op jit(solution)/shard_map/all_to_all | solution.py:77
  704.7 4.4 gather_fusion.1
  709.0 1.5 gather.15
  710.6 6.2 multiply_reduce_fusion
  (28 shorter events, 0.2 us)
Async XLA Ops:
  0.0 364.6 %copy-start = (bf16[1,512,2048]{2,1,0:T(8,128)(2,1)S(1)}, bf16[1,512,2048]{2,1,0:T(8,128)(2,1)}, u32[]{:S(2)}) copy-start(bf16[1,512,2048]{2,1,0:T(8,128)(2,1)} %param.13) | copy-start | bytes 6291460
  247.0 4.5 collective-permute-start
  254.0 2.6 copy-start.3
  254.0 3.3 copy-start.4
  257.3 92.9 %collective-permute-start.1 = (bf16[64,16,2048]{2,1,0:T(8,128)(2,1)}, bf16[64,16,2048]{2,1,0:T(8,128)(2,1)}, u32[]{:S(2)}, u32[]{:S(2)}) collective-permute-start(bf16[64,16,2048]{2,1,0:T(8,128)(2,1)} %pad_maximum_fusion.3), channel_id=1, source_target_pairs={{0,2},{1,3},{2,0},{3,1},{4,6},{5,7},{6,4},{7,5},{8,10},{9,11},{10,... | collective-permute-start | bytes 12582920 | tf_op jit(solution)/shard_map/ppermute | solution.py:15
  257.3 101.2 %copy-start.9 = (bf16[1,2048,512]{2,1,0:T(8,128)(2,1)S(1)}, bf16[1,2048,512]{2,1,0:T(8,128)(2,1)}, u32[]{:S(2)}) copy-start(bf16[1,2048,512]{2,1,0:T(8,128)(2,1)} %param.12) | copy-start | bytes 6291460
  355.3 2.0 copy-start.5
  355.3 3.2 copy-start.6
  387.1 92.1 %collective-permute-start.2 = (bf16[64,16,2048]{2,1,0:T(8,128)(2,1)}, bf16[64,16,2048]{2,1,0:T(8,128)(2,1)}, u32[]{:S(2)}, u32[]{:S(2)}) collective-permute-start(bf16[64,16,2048]{2,1,0:T(8,128)(2,1)} %dynamic-slice_convert_fusion), channel_id=1, source_target_pairs={{0,2},{1,3},{2,0},{3,1},{4,6},{5,7},{6,4},{7,5},{8,10},{9,11},{10,... | collective-permute-start | bytes 12582920 | tf_op jit(solution)/shard_map/ppermute | solution.py:15
  485.1 3.2 copy-start.2
  488.6 4.4 collective-permute-start.3
  498.0 7.8 %copy-start.7 = (s32[128,2]{0,1:T(2,128)S(1)}, s32[128,2]{0,1:T(2,128)}, u32[]{:S(2)}) copy-start(s32[128,2]{0,1:T(2,128)} %param.9) | copy-start | bytes 3076
  498.0 7.9 %copy-start.8 = (f32[128,2]{0,1:T(2,128)S(1)}, f32[128,2]{0,1:T(2,128)}, u32[]{:S(2)}) copy-start(f32[128,2]{0,1:T(2,128)} %param.10) | copy-start | bytes 3076
  498.0 206.7 %all-to-all-start.1 = ((bf16[64,8,2048]{2,1,0:T(8,128)(2,1)}), bf16[64,8,2048]{2,1,0:T(8,128)(2,1)}, u32[]{:S(2)}, u32[]{:S(2)}) async-start(bf16[64,8,2048]{2,1,0:T(8,128)(2,1)} %add_convert_fusion), calls=%async_computation.1 | async-start | bytes 4194304 | tf_op jit(solution)/shard_map/all_to_all | solution.py:77
  704.7 12.1 %copy-start.1 = (bf16[1,512,2048]{2,1,0:T(8,128)(2,1)S(1)}, bf16[1,512,2048]{2,1,0:T(8,128)(2,1)}, u32[]{:S(2)}) copy-start(bf16[1,512,2048]{2,1,0:T(8,128)(2,1)} %param.13) | copy-start | bytes 6291460
where the time goes:
time: 717 us
  waiting for transfers between devices  392 us (55%)
  blocking collectives  233 us (32%)
  other arithmetic  34.3 us (5%)
  local copies, waits for them, and re-layouts  26.5 us (4%)
  matrix products  22.5 us (3%)
  starting transfers between devices  7.97 us (1%)
    all_to_all x1, blocking collectives, body(): lax.all_to_all(pieces, 'ep', split_axis=0, concat_axis=0, tiled=True)  233 us
    all_to_all x1, waiting for transfers between devices, body(): lax.all_to_all(finished, 'ep', split_axis=0, concat_axis=0, tiled=True)  199 us
    ppermute x4, waiting for transfers between devices, swapped(): lax.ppermute(array, axis, [(i, i ^ 1 << bit) for i in range(lax.axis_size...  193 us
    dot_general x1, matrix products, expert_rows(): jnp.einsum('scf,fd->scd', active, down_weight[0], preferred_element_type=...  16.5 us
  transfers between devices with their start and end apart: 5, of which 5 were waited for; matrix products, arithmetic and copies ran while one was open for 0% of the time, Pallas kernels for 0%

commit v1 on v0

v1 whole, which is shorter than its diff:
```python
import functools

import jax
import jax.numpy as jnp
from jax import lax
from jax.experimental import pallas as pl
from jax.experimental.pallas import tpu as pltpu
from jax.sharding import PartitionSpec as P

SPLIT = 4
CORES = 2

EPSILON = 1e-05
clamp_limit = 7.0
sigmoid_slope = 1.702
MESH = pl.DeviceIdType.MESH
F32 = jnp.float32
BF16 = jnp.bfloat16


def kernel(
    devices,
    tokens_ref,
    gain_ref,
    ids_col_ref,
    ids_row_ref,
    weight_col_ref,
    gate_hbm,
    up_hbm,
    down_hbm,
    out_ref,
    ring,
    back,
    meta,
    rows_in,
    own_part,
    sent_part,
    part_in,
    active,
    normed,
    unsort,
    added,
    gate,
    up,
    down,
    load_sem,
    ring_send,
    ring_recv,
    meta_send,
    meta_recv,
    rows_send,
    rows_recv,
    part_send,
    part_recv,
    back_send,
    back_recv,
):
    tok, width = tokens_ref.shape
    hidden = gate.shape[1]
    experts = devices // SPLIT
    side = experts // 2
    cap = min(tok, 2 * tok * ids_col_ref.shape[1] // experts)
    far = devices // CORES // 2
    half = tok // 2
    sizes = [cap * i for i in range(1, half // cap + 1)]
    pair = 2 * cap

    me = lax.axis_index("ep")
    chip = lax.div(me, CORES)
    core = lax.rem(me, CORES)
    sibling = me + 1 - 2 * core
    upper = lax.rem(me + CORES, devices)
    lower = lax.rem(me + devices - CORES, devices)
    parity = lax.rem(chip, 2)
    expert = lax.div(chip, SPLIT // CORES)
    first_code = (expert * cap).astype(F32)

    loads = [
        pltpu.make_async_copy(src.at[0], dst, load_sem.at[i])
        for i, (src, dst) in enumerate(((gate_hbm, gate), (up_hbm, up), (down_hbm, down)))
    ]
    for load in loads:
        load.start()

    def late(way, k):
        odd = lax.rem(chip + k, 2)
        return 1 - odd if way == 0 else odd

    def count(k, offset):
        left = cap * (side - lax.div(k + offset, 2))
        return jnp.minimum(tok, jnp.maximum(left, 0))

    def each_piece(rows, h, act):
        piece = jnp.clip(rows - half * h, 0, half)
        for size in sizes:

            @pl.when(piece == size)
            def _():
                act(size)

    def ring_copy(way, k, h, size):
        span = pl.ds(half * h, size)
        return pltpu.make_async_remote_copy(
            src_ref=ring.at[way, k, span],
            dst_ref=ring.at[way, k + 1, span],
            send_sem=ring_send.at[way, h, k],
            recv_sem=ring_recv.at[way, h, k + 1],
            device_id={"ep": upper if way == 0 else lower},
            device_id_type=MESH,
        )

    def meta_copy(way, k):
        return pltpu.make_async_remote_copy(
            src_ref=meta.at[way, k],
            dst_ref=meta.at[way, k + 1],
            send_sem=meta_send.at[way, k],
            recv_sem=meta_recv.at[way, k + 1],
            device_id={"ep": upper if way == 0 else lower},
            device_id_type=MESH,
        )

    def back_copy(way, k, h, size):
        span = pl.ds(half * h, size)
        return pltpu.make_async_remote_copy(
            src_ref=back.at[way, k, span],
            dst_ref=back.at[way, k - 1, span],
            send_sem=back_send.at[way, h, k],
            recv_sem=back_recv.at[way, h, k - 1],
            device_id={"ep": lower if way == 0 else upper},
            device_id_type=MESH,
        )

    def rows_copy(k):
        return pltpu.make_async_remote_copy(
            src_ref=rows_in.at[k, pl.ds(0, pair)],
            dst_ref=rows_in.at[k, pl.ds(pair, pair)],
            send_sem=rows_send.at[k],
            recv_sem=rows_recv.at[k],
            device_id={"ep": sibling},
            device_id_type=MESH,
        )

    def part_copy(k):
        return pltpu.make_async_remote_copy(
            src_ref=sent_part.at[lax.rem(k, 2)],
            dst_ref=part_in.at[k],
            send_sem=part_send.at[k],
            recv_sem=part_recv.at[k],
            device_id={"ep": sibling},
            device_id_type=MESH,
        )

    shrink = 2 * (side - tok // cap)

    @pl.loop(shrink, far + 1)
    def _(k):
        for way in range(2):
            ring[way, k] = jnp.zeros((tok, width), BF16)
            meta[way, k] = jnp.full(meta.shape[2:], -1.0, F32)

    barrier = pltpu.get_barrier_semaphore()
    for peer in (upper, lower, sibling):
        pl.semaphore_signal(barrier, inc=1, device_id={"ep": peer}, device_id_type=MESH)

    block = min(tok, 32)

    @pl.loop(0, tok // block)
    def _(i):
        span = pl.ds(pl.multiple_of(i * block, block), block)
        values = tokens_ref[span, :].astype(F32)
        center = values - jnp.mean(values, axis=-1, keepdims=True)
        spread = jnp.mean(center * center, axis=-1, keepdims=True)
        normed[span, :] = (center * lax.rsqrt(spread + EPSILON) * gain_ref[...]).astype(BF16)

    def reach(ids, way):
        offset = late(way, 0)
        steps = ids - expert if way == 0 else expert - ids
        steps = jnp.where(steps < 0, steps + experts, steps)
        inside = (steps >= 1 - offset) & (steps <= side - offset)
        return jnp.where(inside, 2 * steps + offset, 0)

    row_index = lax.broadcasted_iota(jnp.int32, (tok, tok), 0)
    col_index = lax.broadcasted_iota(jnp.int32, (tok, tok), 1)
    id_col = [ids_col_ref[:, i : i + 1] for i in range(2)]
    id_row = [ids_row_ref[i : i + 1, :] for i in range(2)]
    weight_col = [weight_col_ref[:, i : i + 1] for i in range(2)]
    code_col = []
    for i in range(2):
        same = ((id_row[0] == id_col[i]) | (id_row[1] == id_col[i])) & (col_index < row_index)
        slot = jnp.sum(jnp.where(same, 1.0, 0.0), axis=1, keepdims=True)
        code_col.append(id_col[i].astype(F32) * float(cap) + slot)
    facts = (code_col[0], code_col[1], weight_col[0], weight_col[1])
    sorts = []
    for way in range(2):
        key_col = jnp.maximum(reach(id_col[0], way), reach(id_col[1], way))
        key_row = jnp.maximum(reach(id_row[0], way), reach(id_row[1], way))
        ahead = (key_row > key_col) | ((key_row == key_col) & (col_index < row_index))
        rank_col = jnp.sum(jnp.where(ahead, 1.0, 0.0), axis=1, keepdims=True).astype(jnp.int32)
        behind = (key_col > key_row) | ((key_col == key_row) & (row_index < col_index))
        rank_row = jnp.sum(jnp.where(behind, 1.0, 0.0), axis=0, keepdims=True).astype(jnp.int32)
        placed = col_index == rank_col
        unsort[way] = jnp.where(placed, 1.0, 0.0).astype(BF16)
        for i, fact in enumerate(facts):
            meta[way, 0, i : i + 1, :] = jnp.sum(
                jnp.where(placed, fact, 0.0), axis=0, keepdims=True
            )
        sorts.append(jnp.where(row_index == rank_row, 1.0, 0.0).astype(BF16))
    for way in range(2):
        ring[way, 0] = jnp.dot(
            sorts[way], normed[...], preferred_element_type=F32
        ).astype(BF16)

    pl.semaphore_wait(barrier, 3)

    def matches(way, k):
        slots = lax.broadcasted_iota(jnp.int32, (cap, tok), 0).astype(F32) + first_code
        return meta[way, k, 0:1, :] == slots, meta[way, k, 1:2, :] == slots

    def onehot(way, k):
        first, second = matches(way, k)
        return jnp.where(first | second, 1.0, 0.0).astype(BF16)

    def pass_on(k, h):
        for way in range(2):
            offset = late(way, k)
            rows = jnp.where(k > 0, count(k - 1, offset), 0)
            each_piece(rows, h, lambda size: ring_copy(way, k - 1, h, size).wait_recv())
            each_piece(count(k, offset), h, lambda size: ring_copy(way, k, h, size).start())
            if h == 0:

                @pl.when(rows > 0)
                def _():
                    meta_copy(way, k - 1).wait_recv()

                @pl.when(count(k, offset) > 0)
                def _():
                    meta_copy(way, k).start()

    def select(k):
        for way in range(2):
            rows_in[k, way * cap : (way + 1) * cap] = jnp.dot(
                onehot(way, k), ring[way, k], preferred_element_type=F32
            ).astype(BF16)
        rows_copy(k).start()

    def hidden_units(k):
        rows_copy(k).wait_recv()
        block_rows = rows_in[k]
        gate_pre = jnp.dot(block_rows, gate[...], preferred_element_type=F32)
        up_pre = jnp.dot(block_rows, up[...], preferred_element_type=F32)
        gate_cut = jnp.minimum(gate_pre, clamp_limit)
        up_cut = jnp.clip(up_pre, -clamp_limit, clamp_limit)
        active[...] = (
            (up_cut + 1.0) * (gate_cut * jax.nn.sigmoid(gate_cut * sigmoid_slope))
        ).astype(BF16)

    def outputs(k):
        slot = lax.rem(k, 2)

        @pl.when(k >= 2)
        def _():
            part_copy(k - 2).wait_send()

        for start in range(0, width, hidden):
            span = slice(start, start + hidden)
            partial = jnp.dot(active[...], down[:, span], preferred_element_type=F32)
            own_part[slot, :, span] = partial[:pair]
            sent_part[slot, :, span] = partial[pair:].astype(BF16)
        part_copy(k).start()

    def weigh(k):
        part_copy(k).wait_recv()
        slot = lax.rem(k, 2)
        for way in range(2):
            first, second = matches(way, k)
            scale = jnp.sum(
                jnp.where(first, meta[way, k, 2:3, :], 0.0)
                + jnp.where(second, meta[way, k, 3:4, :], 0.0),
                axis=1,
                keepdims=True,
            )
            span = slice(way * cap, (way + 1) * cap)
            whole = own_part[slot, span] + part_in[k, span].astype(F32)
            part_in[k, span] = (whole * scale).astype(BF16)

    @pl.loop(0, far + 3)
    def _(k):
        pl.when(k <= far)(lambda: pass_on(k, 0))

        @pl.when((k >= 1) & (k <= far + 1))
        def _():
            @pl.when(k == 1)
            def _():
                for load in loads:
                    load.wait()

            hidden_units(k - 1)

        @pl.when(k <= far)
        def _():
            pass_on(k, 1)
            select(k)

        pl.when((k >= 1) & (k <= far + 1))(lambda: outputs(k - 1))
        pl.when(k >= 2)(lambda: weigh(k - 2))

    def spread_rows(way, k):
        return lax.dot_general(
            onehot(way, k),
            part_in[k, way * cap : (way + 1) * cap],
            (((0,), (0,)), ((), ())),
            preferred_element_type=F32,
        )

    @pl.loop(0, far)
    def _(i):
        k = far - i
        for way in range(2):
            added[way] = spread_rows(way, k).astype(BF16)
        for h in range(2):
            for way in range(2):
                offset = late(way, k)
                held = count(k, offset)
                each_piece(held, h, lambda size: back_copy(way, k + 1, h, size).wait_recv())

                def send(size):
                    span = pl.ds(half * h, size)
                    index = lax.broadcasted_iota(jnp.int32, (size, 1), 0) + half * h
                    before = jnp.where(index < held, back[way, k, span].astype(F32), 0.0)
                    back[way, k, span] = (before + added[way, span].astype(F32)).astype(BF16)
                    back_copy(way, k, h, size).start()

                each_piece(count(k - 1, offset), h, send)

    for h in range(2):
        for way in range(2):
            back_copy(way, 1, h, half).wait_recv()
    total = spread_own = None
    total = lax.dot_general(
        onehot(0, 0),
        part_in[0, 0:cap],
        (((0,), (0,)), ((), ())),
        preferred_element_type=F32,
    )
    own = lax.dot_general(
        unsort[0], total.astype(BF16), (((1,), (0,)), ((), ())), preferred_element_type=F32
    )
    for way in range(2):
        own = own + jnp.dot(unsort[way], back[way, 0], preferred_element_type=F32)
    out_ref[...] = own.astype(BF16)

    @pl.loop(0, far + 1)
    def _(k):
        rows_copy(k).wait_send()
        pl.when(k >= far - 1)(lambda: part_copy(k).wait_send())
        for way in range(2):
            offset = late(way, k)
            rows = count(k, offset)

            @pl.when(rows > 0)
            def _():
                meta_copy(way, k).wait_send()

            for h in range(2):
                each_piece(rows, h, lambda size: ring_copy(way, k, h, size).wait_send())
                sent = jnp.where(k > 0, count(k - 1, offset), 0)
                each_piece(sent, h, lambda size: back_copy(way, k, h, size).wait_send())


def body(tokens, norm_gain, expert_ids, route_weight, gate_weight, up_weight, down_weight):
    devices = lax.axis_size("ep")
    tok, width = tokens.shape
    top_count = expert_ids.shape[1]
    hidden = gate_weight.shape[2]
    experts = devices // SPLIT
    cap = min(tok, 2 * tok * top_count // experts)
    far = devices // CORES // 2
    steps = far + 1
    vmem = pl.BlockSpec(memory_space=pltpu.VMEM)
    hbm = pl.BlockSpec(memory_space=pl.ANY)
    dma = pltpu.SemaphoreType.DMA
    return pl.pallas_call(
        functools.partial(kernel, devices),
        out_shape=jax.ShapeDtypeStruct((tok, width), BF16),
        in_specs=[vmem] * 5 + [hbm] * 3,
        out_specs=vmem,
        scratch_shapes=[
            pltpu.VMEM((2, steps, tok, width), BF16),
            pltpu.VMEM((2, steps, tok, width), BF16),
            pltpu.VMEM((2, steps, 8, tok), F32),
            pltpu.VMEM((steps, 4 * cap, width), BF16),
            pltpu.VMEM((2, 2 * cap, width), F32),
            pltpu.VMEM((2, 2 * cap, width), BF16),
            pltpu.VMEM((steps, 2 * cap, width), BF16),
            pltpu.VMEM((4 * cap, hidden), BF16),
            pltpu.VMEM((tok, width), BF16),
            pltpu.VMEM((2, tok, tok), BF16),
            pltpu.VMEM((2, tok, width), BF16),
            pltpu.VMEM((width, hidden), BF16),
            pltpu.VMEM((width, hidden), BF16),
            pltpu.VMEM((hidden, width), BF16),
            dma((3,)),
            dma((2, 2, steps)),
            dma((2, 2, steps)),
            dma((2, steps)),
            dma((2, steps)),
            dma((steps,)),
            dma((steps,)),
            dma((steps,)),
            dma((steps,)),
            dma((2, 2, steps)),
            dma((2, 2, steps)),
        ],
        compiler_params=pltpu.CompilerParams(
            collective_id=0, has_side_effects=True, vmem_limit_bytes=67043328
        ),
    )(
        tokens,
        norm_gain.reshape(1, width),
        expert_ids,
        expert_ids.T,
        route_weight,
        gate_weight,
        up_weight,
        down_weight,
    )


def solution(mesh):
    placed = (
        P(("grp", "ep"), None),
        P(),
        P(("grp", "ep"), None),
        P(("grp", "ep"), None),
        P("ep", None, None),
        P("ep", None, None),
        P("ep", None, None),
    )
    return jax.shard_map(
        body, mesh=mesh, in_specs=placed, out_specs=P(("grp", "ep"), None), check_vma=False
    )
```

time: 717 us -> 347 us (0.48)
  waiting for transfers between devices: 392 us -> 0 us
  Pallas kernels: 0 us -> 342 us
  blocking collectives: 233 us -> 0 us
  other arithmetic: 34.3 us -> 0 us
  matrix products: 22.5 us -> 0 us
  local copies, waits for them, and re-layouts: 26.5 us -> 4.7 us
  starting transfers between devices: 7.97 us -> 0 us
    pallas_call x0 -> x1, Pallas kernels: none -> 342 us  [body(): pl.pallas_call(functools.partial(kernel, devices), out_shape=jax.ShapeDty...]
    all_to_all x1 -> x0, blocking collectives: 233 us -> none  [body(): lax.all_to_all(pieces, 'ep', split_axis=0, concat_axis=0, tiled=True)]
    all_to_all x1 -> x0, waiting for transfers between devices: 199 us -> none  [body(): lax.all_to_all(finished, 'ep', split_axis=0, concat_axis=0, tiled=True)]
    ppermute x4 -> x0, waiting for transfers between devices: 193 us -> none  [swapped(): lax.ppermute(array, axis, [(i, i ^ 1 << bit) for i in range(lax.axis_size...]
    dot_general x2 -> x0, matrix products: 22.5 us -> none  [the longest x1 16.5 us: expert_rows(): jnp.einsum('scf,fd->scd', active, down_weight[0], preferred_element_type=...]
    select_n x6 -> x0, other arithmetic: 9.34 us -> none  [the longest x2 7.49 us: body(): first_half = jnp.where(upper_bit == 1, partner, gathered)]
    gather x3 -> x0, local copies, waits for them, and re-layouts: 9.24 us -> none  [the longest x2 5.89 us: body(): jnp.take(results, target, axis=0).reshape(tok_rows, top_count, width)]
    reduce_sum x4 -> x0, other arithmetic: 8.86 us -> none  [the longest x1 6.24 us: body(): jnp.sum(route_weight[:, :, None] * picked.astype(jnp.float32), axis=1)]
  transfers between devices with their start and end apart: 5 -> 0, of which waited for: 5 -> 0; matrix products, arithmetic and copies ran while one was open for 0% -> 0% of each run, Pallas kernels for 0% -> 0%
where the time goes in v1:
time: 347 us
  Pallas kernels  342 us (99%)
  local copies, waits for them, and re-layouts  4.7 us (1%)
    pallas_call x1, Pallas kernels, body(): pl.pallas_call(functools.partial(kernel, devices), out_shape=jax.ShapeDty...  342 us

profile of v1, /device:TPU:38, one launch (start us, length us, event | category | flops | bytes accessed | tf_op | source)
XLA Modules:
  0.0 346.8 jit_solution(9046187644194187392)
XLA Ops:
  0.0 1.4 copy.9.weight_col_ref
  1.4 1.4 copy.8.ids_col_ref
  2.8 342.1 %shard_map.73 = bf16[128,2048]{1,0:T(8,128)(2,1)} custom-call(bf16[128,2048]{1,0:T(8,128)(2,1)} %tokens_ref.1, f32[1,2048]{1,0:T(1,128)} %bitcast.2, s32[128,2]{1,0:T(8,128)} %copy.8.ids_col_ref, s32[2,128]{1,0:T(2,128)} %bitcast.3, f32[128,2]{1,0:T(8,128)} %copy.9.weight_col_ref, bf16[1,2048,512]{2,1,0:T(8,128)(2,1)} %gate_hbm.1, ...), custom_call_target="tpu_custom_call" | custom-call | tf_op jit(solution)/shard_map/pallas_call | solution.py:382
  344.9 1.9 copy.11

commit v2 on v0

v2 whole, which is shorter than its diff:
```python
import functools

import jax
import jax.numpy as jnp
from jax import lax
from jax.experimental import pallas as pl
from jax.experimental.pallas import tpu as pltpu
from jax.sharding import PartitionSpec as P

SPLIT = 4
CORES = 2
WAVES = 2
LEAD = 11
SLOTS = 4

EPSILON = 1e-05
clamp_limit = 7.0
sigmoid_slope = 1.702
MESH = pl.DeviceIdType.MESH
F32 = jnp.float32
BF16 = jnp.bfloat16


def left_rows(tok, cap, side, k, offset):
    return min(tok, max(0, cap * (side - (k + offset) // 2)))


def plan(devices, tok, top_count):
    experts = devices // SPLIT
    side = experts // 2
    cap = min(tok, 2 * tok * top_count // experts)
    half = tok // WAVES
    radii, thin = [], []
    for w in range(WAVES):
        hops = range(1, devices // CORES + 1)
        radii.append(max(k for k in hops if left_rows(tok, cap, side, k - 1, 0) > w * half))
        full = (w + 1) * half
        thin.append(min(k for k in hops if left_rows(tok, cap, side, k - 1, 1) < full))
    return experts, side, cap, half, radii, thin


def kernel(
    devices,
    piece,
    tokens_ref,
    gain_ref,
    ids_ref,
    weight_ref,
    gate_hbm,
    up_hbm,
    down_hbm,
    out_ref,
    *scratch,
):
    waves = [scratch[i * 15 : (i + 1) * 15] for i in range(WAVES)]
    active, normed, gate, up, down, load_sem = scratch[WAVES * 15 :]
    (
        ring,
        back,
        meta,
        rows_in,
        own_part,
        sent_part,
        part_in,
        unsort,
        added,
        row_sem,
        part_sem,
        ring_send,
        ring_recv,
        back_send,
        back_recv,
    ) = zip(*waves)
    tok, width = tokens_ref.shape
    hidden = gate.shape[1]
    experts, side, cap, half, radii, thin = plan(devices, tok, ids_ref.shape[0])
    pair = 2 * cap
    pieces = half // piece
    starts = [w * LEAD for w in range(WAVES)]

    me = lax.axis_index("ep")
    chip = lax.div(me, CORES)
    core = lax.rem(me, CORES)
    sibling = me + 1 - 2 * core
    upper = lax.rem(me + CORES, devices)
    lower = lax.rem(me + devices - CORES, devices)
    expert = lax.div(chip, SPLIT // CORES)
    first_code = (expert * cap).astype(F32)

    loads = [
        pltpu.make_async_copy(src.at[0], dst, load_sem.at[i])
        for i, (src, dst) in enumerate(((gate_hbm, gate), (up_hbm, up), (down_hbm, down)))
    ]
    for load in loads:
        load.start()

    def late(way, k):
        odd = lax.rem(chip + k, 2)
        return 1 - odd if way == 0 else odd

    def count(k, offset):
        left = cap * (side - lax.div(k + offset, 2))
        return jnp.minimum(tok, jnp.maximum(left, 0))

    def goes(w, p, rows):
        return rows > w * half + p * piece

    def remote(src, dst, send, recv, peer):
        return pltpu.make_async_remote_copy(
            src_ref=src,
            dst_ref=dst,
            send_sem=send,
            recv_sem=recv,
            device_id={"ep": peer},
            device_id_type=MESH,
        )

    def ring_copy(w, way, k, p):
        span = pl.ds(p * piece, piece)
        return remote(
            ring[w].at[way, k, span],
            ring[w].at[way, k + 1, span],
            ring_send[w].at[way, p, k],
            ring_recv[w].at[way, p, k + 1],
            upper if way == 0 else lower,
        )

    def meta_copy(w, way, k):
        return remote(
            meta[w].at[way, k],
            meta[w].at[way, k + 1],
            ring_send[w].at[way, pieces, k],
            ring_recv[w].at[way, pieces, k + 1],
            upper if way == 0 else lower,
        )

    def back_copy(w, way, k, p):
        span = pl.ds(p * piece, piece)
        return remote(
            back[w].at[way, k, span],
            back[w].at[way, k - 1, span],
            back_send[w].at[way, p, k],
            back_recv[w].at[way, p, k - 1],
            lower if way == 0 else upper,
        )

    def rows_copy(w, k):
        slot = lax.rem(k, SLOTS)
        return remote(
            rows_in[w].at[slot, pl.ds(0, pair)],
            rows_in[w].at[slot, pl.ds(pair, pair)],
            row_sem[w].at[0, k],
            row_sem[w].at[1, k],
            sibling,
        )

    def part_copy(w, k):
        return remote(
            sent_part[w].at[lax.rem(k, 2)],
            part_in[w].at[k],
            part_sem[w].at[0, k],
            part_sem[w].at[1, k],
            sibling,
        )

    for w in range(WAVES):

        @pl.loop(thin[w], radii[w] + 1)
        def _(k):
            for way in range(2):
                ring[w][way, k] = jnp.zeros((half, width), BF16)
                meta[w][way, k] = jnp.full(meta[w].shape[2:], -1.0, F32)

    barrier = pltpu.get_barrier_semaphore()
    for peer in (upper, lower, sibling):
        pl.semaphore_signal(barrier, inc=1, device_id={"ep": peer}, device_id_type=MESH)

    block = min(tok, 32)

    @pl.loop(0, tok // block)
    def _(i):
        span = pl.ds(pl.multiple_of(i * block, block), block)
        values = tokens_ref[span, :].astype(F32)
        center = values - jnp.mean(values, axis=-1, keepdims=True)
        spread = jnp.mean(center * center, axis=-1, keepdims=True)
        normed[span, :] = (center * lax.rsqrt(spread + EPSILON) * gain_ref[...]).astype(BF16)

    def reach(ids, way):
        offset = late(way, 0)
        steps = ids - expert if way == 0 else expert - ids
        steps = jnp.where(steps < 0, steps + experts, steps)
        inside = (steps >= 1 - offset) & (steps <= side - offset)
        return jnp.where(inside, 2 * steps + offset, 0).astype(F32)

    row_index = lax.broadcasted_iota(jnp.int32, (tok, tok), 0)
    col_index = lax.broadcasted_iota(jnp.int32, (tok, tok), 1)
    diagonal = row_index == col_index

    def as_column(row):
        return jnp.sum(jnp.where(diagonal, row, 0.0), axis=1, keepdims=True)

    id_row = [ids_ref[i : i + 1, :] for i in range(2)]
    code_row = [ids.astype(F32) for ids in id_row]
    code_col = [as_column(code) for code in code_row]
    facts = []
    for i in range(2):
        same = (code_row[0] == code_col[i]) | (code_row[1] == code_col[i])
        slot = jnp.sum(
            jnp.where(same & (col_index < row_index), 1.0, 0.0), axis=1, keepdims=True
        )
        facts.append(code_col[i] * float(cap) + slot)
    facts += [as_column(weight_ref[i : i + 1, :]) for i in range(2)]
    for way in range(2):
        key_row = jnp.maximum(reach(id_row[0], way), reach(id_row[1], way))
        key_col = as_column(key_row)
        ahead = (key_row > key_col) | ((key_row == key_col) & (col_index < row_index))
        rank_col = jnp.sum(jnp.where(ahead, 1.0, 0.0), axis=1, keepdims=True).astype(jnp.int32)
        behind = (key_col > key_row) | ((key_col == key_row) & (row_index < col_index))
        rank_row = jnp.sum(jnp.where(behind, 1.0, 0.0), axis=0, keepdims=True).astype(jnp.int32)
        sort = jnp.where(row_index == rank_row, 1.0, 0.0).astype(BF16)
        ordered = jnp.dot(sort, normed[...], preferred_element_type=F32).astype(BF16)
        for w in range(WAVES):
            placed = col_index + w * half == rank_col
            unsort[w][way] = jnp.where(placed, 1.0, 0.0).astype(BF16)
            for i, fact in enumerate(facts):
                meta[w][way, 0, i : i + 1, :] = jnp.sum(
                    jnp.where(placed, fact, 0.0), axis=0, keepdims=True
                )
            ring[w][way, 0] = ordered[w * half : (w + 1) * half]

    pl.semaphore_wait(barrier, 3)

    def matches(w, way, k):
        slots = lax.broadcasted_iota(jnp.int32, (cap, half), 0).astype(F32) + first_code
        return meta[w][way, k, 0:1, 0:half] == slots, meta[w][way, k, 1:2, 0:half] == slots

    def onehot(w, way, k):
        first, second = matches(w, way, k)
        return jnp.where(first | second, 1.0, 0.0).astype(BF16)

    def pass_on(w, k):
        for way in range(2):
            offset = late(way, k)
            came = (k > 0) & goes(w, 0, count(k - 1, offset))
            pl.when(came)(lambda: meta_copy(w, way, k - 1).wait_recv())
            pl.when(goes(w, 0, count(k, offset)))(lambda: meta_copy(w, way, k).start())
        for p in range(pieces):
            for way in range(2):
                offset = late(way, k)
                came = (k > 0) & goes(w, p, count(k - 1, offset))
                pl.when(came)(lambda: ring_copy(w, way, k - 1, p).wait_recv())
                pl.when(goes(w, p, count(k, offset)))(lambda: ring_copy(w, way, k, p).start())

    def select(w, k):
        slot = lax.rem(k, SLOTS)
        pl.when(k >= SLOTS)(lambda: rows_copy(w, k - SLOTS).wait_send())
        for way in range(2):
            rows_in[w][slot, way * cap : (way + 1) * cap] = jnp.dot(
                onehot(w, way, k), ring[w][way, k], preferred_element_type=F32
            ).astype(BF16)
        rows_copy(w, k).start()

    def expert_rows(w, k):
        rows_copy(w, k).wait_recv()
        block_rows = rows_in[w][lax.rem(k, SLOTS)]
        gate_pre = jnp.dot(block_rows, gate[...], preferred_element_type=F32)
        up_pre = jnp.dot(block_rows, up[...], preferred_element_type=F32)
        gate_cut = jnp.minimum(gate_pre, clamp_limit)
        up_cut = jnp.clip(up_pre, -clamp_limit, clamp_limit)
        active[...] = (
            (up_cut + 1.0) * (gate_cut * jax.nn.sigmoid(gate_cut * sigmoid_slope))
        ).astype(BF16)
        slot = lax.rem(k, 2)
        pl.when(k >= 2)(lambda: part_copy(w, k - 2).wait_send())
        for start in range(0, width, hidden):
            span = slice(start, start + hidden)
            partial = jnp.dot(active[...], down[:, span], preferred_element_type=F32)
            own_part[w][slot, :, span] = partial[:pair]
            sent_part[w][slot, :, span] = partial[pair:].astype(BF16)
        part_copy(w, k).start()

    def weigh(w, k):
        part_copy(w, k).wait_recv()
        slot = lax.rem(k, 2)
        for way in range(2):
            first, second = matches(w, way, k)
            scale = jnp.sum(
                jnp.where(first, meta[w][way, k, 2:3, 0:half], 0.0)
                + jnp.where(second, meta[w][way, k, 3:4, 0:half], 0.0),
                axis=1,
                keepdims=True,
            )
            span = slice(way * cap, (way + 1) * cap)
            whole = own_part[w][slot, span] + part_in[w][k, span].astype(F32)
            part_in[w][k, span] = (whole * scale).astype(BF16)

    def spread_rows(w, way, k):
        return lax.dot_general(
            onehot(w, way, k),
            part_in[w][k, way * cap : (way + 1) * cap],
            (((0,), (0,)), ((), ())),
            preferred_element_type=F32,
        ).astype(BF16)

    def bring_back(w, k):
        for way in range(2):
            added[w][way] = spread_rows(w, way, k)
        for p in range(pieces):
            for way in range(2):
                offset = late(way, k)
                held = goes(w, p, count(k, offset))
                pl.when(held)(lambda: back_copy(w, way, k + 1, p).wait_recv())

                @pl.when(goes(w, p, count(k - 1, offset)))
                def _():
                    span = pl.ds(p * piece, piece)
                    before = jnp.where(held, back[w][way, k, span].astype(F32), 0.0)
                    back[w][way, k, span] = (before + added[w][way, span].astype(F32)).astype(BF16)
                    back_copy(w, way, k, p).start()

    def within(value, low, high):
        return (value >= low) & (value <= high)

    @pl.loop(0, max(s + 2 * r for s, r in zip(starts, radii)) + 3)
    def _(i):
        for w in range(WAVES):
            k = i - starts[w]
            pl.when(within(k, 0, radii[w]))(lambda: pass_on(w, k))
            home = 2 * radii[w] + 3 - k
            pl.when(within(home, 1, radii[w]))(lambda: bring_back(w, home))

        @pl.when(i == 1)
        def _():
            for load in loads:
                load.wait()

        for w in range(WAVES):
            k = i - starts[w]
            pl.when(within(k, 1, radii[w] + 1))(lambda: expert_rows(w, k - 1))
            pl.when(within(k, 0, radii[w]))(lambda: select(w, k))
            pl.when(within(k, 2, radii[w] + 2))(lambda: weigh(w, k - 2))

    total = None
    for w in range(WAVES):
        for p in range(pieces):
            for way in range(2):
                back_copy(w, way, 1, p).wait_recv()
        for way, rows in ((0, spread_rows(w, 0, 0)), (0, back[w][0, 0]), (1, back[w][1, 0])):
            share = jnp.dot(unsort[w][way, :, 0:half], rows, preferred_element_type=F32)
            total = share if total is None else total + share
    out_ref[...] = total.astype(BF16)

    for w in range(WAVES):

        @pl.loop(0, radii[w] + 1)
        def _(k):
            pl.when(k > radii[w] - SLOTS)(lambda: rows_copy(w, k).wait_send())
            pl.when(k > radii[w] - 2)(lambda: part_copy(w, k).wait_send())
            for way in range(2):
                offset = late(way, k)
                rows = count(k, offset)
                pl.when(goes(w, 0, rows))(lambda: meta_copy(w, way, k).wait_send())
                for p in range(pieces):
                    pl.when(goes(w, p, rows))(lambda: ring_copy(w, way, k, p).wait_send())
                    sent = (k > 0) & goes(w, p, count(k - 1, offset))
                    pl.when(sent)(lambda: back_copy(w, way, k, p).wait_send())


def body(tokens, norm_gain, expert_ids, route_weight, gate_weight, up_weight, down_weight):
    devices = lax.axis_size("ep")
    tok, width = tokens.shape
    hidden = gate_weight.shape[2]
    experts, side, cap, half, radii, thin = plan(devices, tok, expert_ids.shape[1])
    piece = cap
    vmem = pl.BlockSpec(memory_space=pltpu.VMEM)
    hbm = pl.BlockSpec(memory_space=pl.ANY)
    dma = pltpu.SemaphoreType.DMA
    scratch = []
    for radius in radii:
        steps = radius + 1
        scratch += [
            pltpu.VMEM((2, steps, half, width), BF16),
            pltpu.VMEM((2, steps, half, width), BF16),
            pltpu.VMEM((2, steps, 8, tok), F32),
            pltpu.VMEM((SLOTS, 4 * cap, width), BF16),
            pltpu.VMEM((2, 2 * cap, width), F32),
            pltpu.VMEM((2, 2 * cap, width), BF16),
            pltpu.VMEM((steps, 2 * cap, width), BF16),
            pltpu.VMEM((2, tok, tok), BF16),
            pltpu.VMEM((2, half, width), BF16),
            dma((2, steps)),
            dma((2, steps)),
            dma((2, half // piece + 1, steps)),
            dma((2, half // piece + 1, steps)),
            dma((2, half // piece, steps)),
            dma((2, half // piece, steps)),
        ]
    scratch += [
        pltpu.VMEM((4 * cap, hidden), BF16),
        pltpu.VMEM((tok, width), BF16),
        pltpu.VMEM((width, hidden), BF16),
        pltpu.VMEM((width, hidden), BF16),
        pltpu.VMEM((hidden, width), BF16),
        dma((3,)),
    ]
    return pl.pallas_call(
        functools.partial(kernel, devices, piece),
        out_shape=jax.ShapeDtypeStruct((tok, width), BF16),
        in_specs=[vmem] * 4 + [hbm] * 3,
        out_specs=vmem,
        scratch_shapes=scratch,
        compiler_params=pltpu.CompilerParams(
            collective_id=0, has_side_effects=True, vmem_limit_bytes=67043328
        ),
    )(
        tokens,
        norm_gain.reshape(1, width),
        expert_ids.T,
        route_weight.T,
        gate_weight,
        up_weight,
        down_weight,
    )


def solution(mesh):
    placed = (
        P(("grp", "ep"), None),
        P(),
        P(("grp", "ep"), None),
        P(("grp", "ep"), None),
        P("ep", None, None),
        P("ep", None, None),
        P("ep", None, None),
    )
    return jax.shard_map(
        body, mesh=mesh, in_specs=placed, out_specs=P(("grp", "ep"), None), check_vma=False
    )
```

time: 717 us -> 332 us (0.46)
  waiting for transfers between devices: 392 us -> 0 us
  Pallas kernels: 0 us -> 330 us
  blocking collectives: 233 us -> 0 us
  other arithmetic: 34.3 us -> 0 us
  local copies, waits for them, and re-layouts: 26.5 us -> 1.88 us
  matrix products: 22.5 us -> 0 us
  starting transfers between devices: 7.97 us -> 0 us
    pallas_call x0 -> x1, Pallas kernels: none -> 330 us  [body(): pl.pallas_call(functools.partial(kernel, devices, piece), out_shape=jax.S...]
    all_to_all x1 -> x0, blocking collectives: 233 us -> none  [body(): lax.all_to_all(pieces, 'ep', split_axis=0, concat_axis=0, tiled=True)]
    all_to_all x1 -> x0, waiting for transfers between devices: 199 us -> none  [body(): lax.all_to_all(finished, 'ep', split_axis=0, concat_axis=0, tiled=True)]
    ppermute x4 -> x0, waiting for transfers between devices: 193 us -> none  [swapped(): lax.ppermute(array, axis, [(i, i ^ 1 << bit) for i in range(lax.axis_size...]
    dot_general x2 -> x0, matrix products: 22.5 us -> none  [the longest x1 16.5 us: expert_rows(): jnp.einsum('scf,fd->scd', active, down_weight[0], preferred_element_type=...]
    select_n x6 -> x0, other arithmetic: 9.34 us -> none  [the longest x2 7.49 us: body(): first_half = jnp.where(upper_bit == 1, partner, gathered)]
    gather x3 -> x0, local copies, waits for them, and re-layouts: 9.24 us -> none  [the longest x2 5.89 us: body(): jnp.take(results, target, axis=0).reshape(tok_rows, top_count, width)]
    reduce_sum x4 -> x0, other arithmetic: 8.86 us -> none  [the longest x1 6.24 us: body(): jnp.sum(route_weight[:, :, None] * picked.astype(jnp.float32), axis=1)]
  transfers between devices with their start and end apart: 5 -> 0, of which waited for: 5 -> 0; matrix products, arithmetic and copies ran while one was open for 0% -> 0% of each run, Pallas kernels for 0% -> 0%
where the time goes in v2:
time: 332 us
  Pallas kernels  330 us (99%)
    pallas_call x1, Pallas kernels, body(): pl.pallas_call(functools.partial(kernel, devices, piece), out_shape=jax.S...  330 us

profile of v2, /device:TPU:38, one launch (start us, length us, event | category | flops | bytes accessed | tf_op | source)
XLA Modules:
  0.0 332.1 jit_solution(7557149859961778769)
XLA Ops:
  0.0 330.2 %shard_map.73 = bf16[128,2048]{1,0:T(8,128)(2,1)} custom-call(bf16[128,2048]{1,0:T(8,128)(2,1)} %tokens_ref.1, f32[1,2048]{1,0:T(1,128)} %bitcast.3, s32[2,128]{1,0:T(2,128)} %bitcast.4, f32[2,128]{1,0:T(2,128)} %bitcast.5, bf16[1,2048,512]{2,1,0:T(8,128)(2,1)} %gate_hbm.1, bf16[1,2048,512]{2,1,0:T(8,128)(2,1)} %up_hbm.1, bf16[1,512,2048]{2,1,0:T(8,128)(2,1)} %down_hbm.1), custom_call_target="tpu_custom_call" | custom-call | tf_op jit(solution)/shard_map/pallas_call | solution.py:406
  330.3 1.9 copy.9

commit v3 on v2

--- a/solution.py
+++ b/solution.py
@@ -42,7 +42,7 @@
 def kernel(
     devices,
     piece,
-    tokens_ref,
+    tokens_hbm,
     gain_ref,
     ids_ref,
     weight_ref,
@@ -52,8 +52,8 @@
     out_ref,
     *scratch,
 ):
-    waves = [scratch[i * 15 : (i + 1) * 15] for i in range(WAVES)]
-    active, normed, gate, up, down, load_sem = scratch[WAVES * 15 :]
+    waves = [scratch[i * 14 : (i + 1) * 14] for i in range(WAVES)]
+    active, tokens, normed, sort, rows, gate, up, down, load_sem = scratch[WAVES * 14 :]
     (
         ring,
         back,
@@ -62,7 +62,6 @@
         own_part,
         sent_part,
         part_in,
-        unsort,
         added,
         row_sem,
         part_sem,
@@ -71,7 +70,7 @@
         back_send,
         back_recv,
     ) = zip(*waves)
-    tok, width = tokens_ref.shape
+    tok, width = tokens.shape
     hidden = gate.shape[1]
     experts, side, cap, half, radii, thin = plan(devices, tok, ids_ref.shape[0])
     pair = 2 * cap
@@ -87,6 +86,8 @@
     expert = lax.div(chip, SPLIT // CORES)
     first_code = (expert * cap).astype(F32)
 
+    fetch = pltpu.make_async_copy(tokens_hbm, tokens, load_sem.at[3])
+    fetch.start()
     loads = [
         pltpu.make_async_copy(src.at[0], dst, load_sem.at[i])
         for i, (src, dst) in enumerate(((gate_hbm, gate), (up_hbm, up), (down_hbm, down)))
@@ -175,16 +176,6 @@
     for peer in (upper, lower, sibling):
         pl.semaphore_signal(barrier, inc=1, device_id={"ep": peer}, device_id_type=MESH)
 
-    block = min(tok, 32)
-
-    @pl.loop(0, tok // block)
-    def _(i):
-        span = pl.ds(pl.multiple_of(i * block, block), block)
-        values = tokens_ref[span, :].astype(F32)
-        center = values - jnp.mean(values, axis=-1, keepdims=True)
-        spread = jnp.mean(center * center, axis=-1, keepdims=True)
-        normed[span, :] = (center * lax.rsqrt(spread + EPSILON) * gain_ref[...]).astype(BF16)
-
     def reach(ids, way):
         offset = late(way, 0)
         steps = ids - expert if way == 0 else expert - ids
@@ -192,41 +183,63 @@
         inside = (steps >= 1 - offset) & (steps <= side - offset)
         return jnp.where(inside, 2 * steps + offset, 0).astype(F32)
 
+    def across(left, right):
+        return lax.dot_general(left, right, (((1,), (1,)), ((), ())), preferred_element_type=F32)
+
     row_index = lax.broadcasted_iota(jnp.int32, (tok, tok), 0)
     col_index = lax.broadcasted_iota(jnp.int32, (tok, tok), 1)
-    diagonal = row_index == col_index
-
-    def as_column(row):
-        return jnp.sum(jnp.where(diagonal, row, 0.0), axis=1, keepdims=True)
-
-    id_row = [ids_ref[i : i + 1, :] for i in range(2)]
-    code_row = [ids.astype(F32) for ids in id_row]
-    code_col = [as_column(code) for code in code_row]
-    facts = []
+    earlier = row_index < col_index
+    ids = [ids_ref[i : i + 1, :] for i in range(2)]
+    id_row = [each.astype(F32) for each in ids]
+    key_row = [jnp.maximum(reach(ids[0], way), reach(ids[1], way)) for way in range(2)]
+    rows[...] = jnp.zeros_like(rows)
+    for i, row in enumerate((*id_row, *key_row)):
+        rows[i : i + 1, :] = row
+    identity = jnp.where(row_index == col_index, 1.0, 0.0).astype(BF16)
+    columns = across(identity, rows[...].astype(BF16))
+    id_col = [columns[:, i : i + 1] for i in range(2)]
+    for way in range(2):
+        key_col = columns[:, 2 + way : 3 + way]
+        behind = (key_col > key_row[way]) | ((key_col == key_row[way]) & earlier)
+        rank = jnp.sum(jnp.where(behind, 1.0, 0.0), axis=0, keepdims=True).astype(jnp.int32)
+        sort[way] = jnp.where(row_index == rank, 1.0, 0.0).astype(BF16)
     for i in range(2):
-        same = (code_row[0] == code_col[i]) | (code_row[1] == code_col[i])
-        slot = jnp.sum(
-            jnp.where(same & (col_index < row_index), 1.0, 0.0), axis=1, keepdims=True
-        )
-        facts.append(code_col[i] * float(cap) + slot)
-    facts += [as_column(weight_ref[i : i + 1, :]) for i in range(2)]
-    for way in range(2):
-        key_row = jnp.maximum(reach(id_row[0], way), reach(id_row[1], way))
-        key_col = as_column(key_row)
-        ahead = (key_row > key_col) | ((key_row == key_col) & (col_index < row_index))
-        rank_col = jnp.sum(jnp.where(ahead, 1.0, 0.0), axis=1, keepdims=True).astype(jnp.int32)
-        behind = (key_col > key_row) | ((key_col == key_row) & (row_index < col_index))
-        rank_row = jnp.sum(jnp.where(behind, 1.0, 0.0), axis=0, keepdims=True).astype(jnp.int32)
-        sort = jnp.where(row_index == rank_row, 1.0, 0.0).astype(BF16)
-        ordered = jnp.dot(sort, normed[...], preferred_element_type=F32).astype(BF16)
-        for w in range(WAVES):
-            placed = col_index + w * half == rank_col
-            unsort[w][way] = jnp.where(placed, 1.0, 0.0).astype(BF16)
-            for i, fact in enumerate(facts):
-                meta[w][way, 0, i : i + 1, :] = jnp.sum(
-                    jnp.where(placed, fact, 0.0), axis=0, keepdims=True
+        same = ((id_col[0] == id_row[i]) | (id_col[1] == id_row[i])) & earlier
+        rows[i : i + 1, :] = id_row[i]
+        rows[2 + i : 3 + i, :] = jnp.sum(jnp.where(same, 1.0, 0.0), axis=0, keepdims=True)
+        rest = weight_ref[i : i + 1, :]
+        for j in range(3):
+            high = rest.astype(BF16).astype(F32)
+            rows[4 + 3 * i + j : 5 + 3 * i + j, :] = high
+            rest = rest - high
+    facts = rows[...].astype(BF16)
+    for w in range(WAVES):
+        for way in range(2):
+            sorted_facts = across(facts, sort[way, w * half : (w + 1) * half, :])
+            fact = [sorted_facts[i : i + 1] for i in range(10)]
+            meta[w][way, 0] = jnp.full(meta[w].shape[2:], -1.0, F32)
+            for i in range(2):
+                meta[w][way, 0, i : i + 1, 0:half] = fact[i] * float(cap) + fact[2 + i]
+                meta[w][way, 0, 2 + i : 3 + i, 0:half] = (
+                    fact[4 + 3 * i] + fact[5 + 3 * i] + fact[6 + 3 * i]
                 )
-            ring[w][way, 0] = ordered[w * half : (w + 1) * half]
+
+    fetch.wait()
+    block = min(tok, 16)
+    for start in range(0, tok, block):
+        span = slice(start, start + block)
+        values = tokens[span, :].astype(F32)
+        center = values - jnp.mean(values, axis=-1, keepdims=True)
+        spread = jnp.mean(center * center, axis=-1, keepdims=True)
+        normed[span, :] = (center * lax.rsqrt(spread + EPSILON) * gain_ref[...]).astype(BF16)
+
+    def put_in_order(w):
+        for way in range(2):
+            ring[w][way, 0] = jnp.dot(
+                sort[way, w * half : (w + 1) * half, :], normed[...], preferred_element_type=F32
+            ).astype(BF16)
+
+    put_in_order(0)
 
     pl.semaphore_wait(barrier, 3)
 
@@ -333,6 +346,8 @@
         def _():
             for load in loads:
                 load.wait()
+            for w in range(1, WAVES):
+                put_in_order(w)
 
         for w in range(WAVES):
             k = i - starts[w]
@@ -345,8 +360,13 @@
         for p in range(pieces):
             for way in range(2):
                 back_copy(w, way, 1, p).wait_recv()
-        for way, rows in ((0, spread_rows(w, 0, 0)), (0, back[w][0, 0]), (1, back[w][1, 0])):
-            share = jnp.dot(unsort[w][way, :, 0:half], rows, preferred_element_type=F32)
+        for way, part in ((0, spread_rows(w, 0, 0)), (0, back[w][0, 0]), (1, back[w][1, 0])):
+            share = lax.dot_general(
+                sort[way, w * half : (w + 1) * half, :],
+                part,
+                (((0,), (0,)), ((), ())),
+                preferred_element_type=F32,
+            )
             total = share if total is None else total + share
     out_ref[...] = total.astype(BF16)
 
@@ -386,7 +406,6 @@
             pltpu.VMEM((2, 2 * cap, width), F32),
             pltpu.VMEM((2, 2 * cap, width), BF16),
             pltpu.VMEM((steps, 2 * cap, width), BF16),
-            pltpu.VMEM((2, tok, tok), BF16),
             pltpu.VMEM((2, half, width), BF16),
             dma((2, steps)),
             dma((2, steps)),
@@ -398,15 +417,18 @@
     scratch += [
         pltpu.VMEM((4 * cap, hidden), BF16),
         pltpu.VMEM((tok, width), BF16),
+        pltpu.VMEM((tok, width), BF16),
+        pltpu.VMEM((2, tok, tok), BF16),
+        pltpu.VMEM((16, tok), F32),
         pltpu.VMEM((width, hidden), BF16),
         pltpu.VMEM((width, hidden), BF16),
         pltpu.VMEM((hidden, width), BF16),
-        dma((3,)),
+        dma((4,)),
     ]
     return pl.pallas_call(
         functools.partial(kernel, devices, piece),
         out_shape=jax.ShapeDtypeStruct((tok, width), BF16),
-        in_specs=[vmem] * 4 + [hbm] * 3,
+        in_specs=[hbm] + [vmem] * 3 + [hbm] * 3,
         out_specs=vmem,
         scratch_shapes=scratch,
         compiler_params=pltpu.CompilerParams(

time: 332 us -> 332 us (level)
  no operation moved by 1% of the time
where the time goes in v3:
time: 332 us
  Pallas kernels  330 us (99%)
    pallas_call x1, Pallas kernels, body(): pl.pallas_call(functools.partial(kernel, devices, piece), out_shape=jax.S...  330 us

profile of v3, /device:TPU:38, one launch (start us, length us, event | category | flops | bytes accessed | tf_op | source)
XLA Modules:
  0.0 331.8 jit_solution(11382003615071060172)
XLA Ops:
  0.0 329.9 %shard_map.73 = bf16[128,2048]{1,0:T(8,128)(2,1)} custom-call(bf16[128,2048]{1,0:T(8,128)(2,1)} %tokens_hbm.1, f32[1,2048]{1,0:T(1,128)} %bitcast.3, s32[2,128]{1,0:T(2,128)} %bitcast.4, f32[2,128]{1,0:T(2,128)} %bitcast.5, bf16[1,2048,512]{2,1,0:T(8,128)(2,1)} %gate_hbm.1, bf16[1,2048,512]{2,1,0:T(8,128)(2,1)} %up_hbm.1, bf16[1,512,2048]{2,1,0:T(8,128)(2,1)} %down_hbm.1), custom_call_target="tpu_custom_call" | custom-call | tf_op jit(solution)/shard_map/pallas_call | solution.py:428
  329.9 1.9 copy.9

commit v4 on v3

--- a/solution.py
+++ b/solution.py
@@ -12,6 +12,7 @@
 WAVES = 2
 LEAD = 11
 SLOTS = 4
+PARTS = 2
 
 EPSILON = 1e-05
 clamp_limit = 7.0
@@ -52,8 +53,8 @@
     out_ref,
     *scratch,
 ):
-    waves = [scratch[i * 14 : (i + 1) * 14] for i in range(WAVES)]
-    active, tokens, normed, sort, rows, gate, up, down, load_sem = scratch[WAVES * 14 :]
+    waves = [scratch[i * 15 : (i + 1) * 15] for i in range(WAVES)]
+    active, tokens, normed, sort, rows, gate, up, down, load_sem = scratch[WAVES * 15 :]
     (
         ring,
         back,
@@ -66,6 +67,7 @@
         row_sem,
         part_sem,
         ring_send,
+        meta_send,
         ring_recv,
         back_send,
         back_recv,
@@ -86,14 +88,16 @@
     expert = lax.div(chip, SPLIT // CORES)
     first_code = (expert * cap).astype(F32)
 
-    fetch = pltpu.make_async_copy(tokens_hbm, tokens, load_sem.at[3])
+    fetch = pltpu.make_async_copy(tokens_hbm, tokens, load_sem.at[0])
     fetch.start()
-    loads = [
-        pltpu.make_async_copy(src.at[0], dst, load_sem.at[i])
-        for i, (src, dst) in enumerate(((gate_hbm, gate), (up_hbm, up), (down_hbm, down)))
-    ]
-    for load in loads:
-        load.start()
+    loads = []
+    for src, dst in ((gate_hbm, gate), (up_hbm, up), (down_hbm, down)):
+        depth = dst.shape[0] // PARTS
+        for j in range(PARTS):
+            span = pl.ds(j * depth, depth)
+            loads.append(
+                pltpu.make_async_copy(src.at[0, span], dst.at[span], load_sem.at[len(loads) + 1])
+            )
 
     def late(way, k):
         odd = lax.rem(chip + k, 2)
@@ -102,6 +106,19 @@
     def count(k, offset):
         left = cap * (side - lax.div(k + offset, 2))
         return jnp.minimum(tok, jnp.maximum(left, 0))
+
+    def sent_rows(w, first):
+        return [
+            min(half, max(0, left_rows(tok, cap, side, k, (k + first) % 2) - w * half))
+            for k in range(radii[w])
+        ]
+
+    def sent_slots(w, first):
+        assert sum(sent_rows(w, first)) % half == 0
+        return sum(sent_rows(w, first)) // half
+
+    def sent_hops(w, first):
+        return sum(r > 0 for r in sent_rows(w, first))
 
     def goes(w, p, rows):
         return rows > w * half + p * piece
@@ -121,8 +138,8 @@
         return remote(
             ring[w].at[way, k, span],
             ring[w].at[way, k + 1, span],
-            ring_send[w].at[way, p, k],
-            ring_recv[w].at[way, p, k + 1],
+            ring_send[w].at[way],
+            ring_recv[w].at[way, p, lax.rem(k + 1, SLOTS)],
             upper if way == 0 else lower,
         )
 
@@ -130,8 +147,8 @@
         return remote(
             meta[w].at[way, k],
             meta[w].at[way, k + 1],
-            ring_send[w].at[way, pieces, k],
-            ring_recv[w].at[way, pieces, k + 1],
+            meta_send[w].at[way],
+            ring_recv[w].at[way, pieces, lax.rem(k + 1, SLOTS)],
             upper if way == 0 else lower,
         )
 
@@ -140,8 +157,8 @@
         return remote(
             back[w].at[way, k, span],
             back[w].at[way, k - 1, span],
-            back_send[w].at[way, p, k],
-            back_recv[w].at[way, p, k - 1],
+            back_send[w].at[way],
+            back_recv[w].at[way, p, lax.rem(k - 1, SLOTS)],
             lower if way == 0 else upper,
         )
 
@@ -150,17 +167,18 @@
         return remote(
             rows_in[w].at[slot, pl.ds(0, pair)],
             rows_in[w].at[slot, pl.ds(pair, pair)],
-            row_sem[w].at[0, k],
-            row_sem[w].at[1, k],
+            row_sem[w].at[0, slot],
+            row_sem[w].at[1, slot],
             sibling,
         )
 
     def part_copy(w, k):
+        slot = lax.rem(k, SLOTS)
         return remote(
             sent_part[w].at[lax.rem(k, 2)],
             part_in[w].at[k],
-            part_sem[w].at[0, k],
-            part_sem[w].at[1, k],
+            part_sem[w].at[0, slot],
+            part_sem[w].at[1, slot],
             sibling,
         )
 
@@ -225,6 +243,8 @@
                 )
 
     fetch.wait()
+    for load in loads:
+        load.start()
     block = min(tok, 16)
     for start in range(0, tok, block):
         span = slice(start, start + block)
@@ -370,20 +390,24 @@
             total = share if total is None else total + share
     out_ref[...] = total.astype(BF16)
 
+    def finish(w, way, first):
+        peer = upper if way == 0 else lower
+        for buf, send, recv, slots in (
+            (ring[w], ring_send[w], ring_recv[w], sent_slots(w, first)),
+            (meta[w], meta_send[w], ring_recv[w], sent_hops(w, first)),
+            (back[w], back_send[w], back_recv[w], sent_slots(w, 1 - first)),
+        ):
+            span = buf.at[way, pl.ds(0, slots)]
+            remote(span, span, send.at[way], recv.at[way, 0, 0], peer).wait_send()
+
     for w in range(WAVES):
-
-        @pl.loop(0, radii[w] + 1)
-        def _(k):
-            pl.when(k > radii[w] - SLOTS)(lambda: rows_copy(w, k).wait_send())
-            pl.when(k > radii[w] - 2)(lambda: part_copy(w, k).wait_send())
-            for way in range(2):
-                offset = late(way, k)
-                rows = count(k, offset)
-                pl.when(goes(w, 0, rows))(lambda: meta_copy(w, way, k).wait_send())
-                for p in range(pieces):
-                    pl.when(goes(w, p, rows))(lambda: ring_copy(w, way, k, p).wait_send())
-                    sent = (k > 0) & goes(w, p, count(k - 1, offset))
-                    pl.when(sent)(lambda: back_copy(w, way, k, p).wait_send())
+        for k in range(radii[w] + 1 - SLOTS, radii[w] + 1):
+            rows_copy(w, k).wait_send()
+        for k in range(radii[w] - 1, radii[w] + 1):
+            part_copy(w, k).wait_send()
+        for way in range(2):
+            for first in range(2):
+                pl.when(late(way, 0) == first)(lambda: finish(w, way, first))
 
 
 def body(tokens, norm_gain, expert_ids, route_weight, gate_weight, up_weight, down_weight):
@@ -407,12 +431,13 @@
             pltpu.VMEM((2, 2 * cap, width), BF16),
             pltpu.VMEM((steps, 2 * cap, width), BF16),
             pltpu.VMEM((2, half, width), BF16),
-            dma((2, steps)),
-            dma((2, steps)),
-            dma((2, half // piece + 1, steps)),
-            dma((2, half // piece + 1, steps)),
-            dma((2, half // piece, steps)),
-            dma((2, half // piece, steps)),
+            dma((2, SLOTS)),
+            dma((2, SLOTS)),
+            dma((2,)),
+            dma((2,)),
+            dma((2, half // piece + 1, SLOTS)),
+            dma((2,)),
+            dma((2, half // piece, SLOTS)),
         ]
     scratch += [
         pltpu.VMEM((4 * cap, hidden), BF16),
@@ -423,7 +448,7 @@
         pltpu.VMEM((width, hidden), BF16),
         pltpu.VMEM((width, hidden), BF16),
         pltpu.VMEM((hidden, width), BF16),
-        dma((4,)),
+        dma((3 * PARTS + 1,)),
     ]
     return pl.pallas_call(
         functools.partial(kernel, devices, piece),

time: 332 us -> 325 us (0.979)
  Pallas kernels: 330 us -> 323 us
    pallas_call x1, Pallas kernels: 330 us -> 323 us  [body(): pl.pallas_call(functools.partial(kernel, devices, piece), out_shape=jax.S...]
where the time goes in v4:
time: 325 us
  Pallas kernels  323 us (99%)
    pallas_call x1, Pallas kernels, body(): pl.pallas_call(functools.partial(kernel, devices, piece), out_shape=jax.S...  323 us

profile of v4, /device:TPU:38, one launch (start us, length us, event | category | flops | bytes accessed | tf_op | source)
XLA Modules:
  0.0 325.0 jit_solution(10773762864443894238)
XLA Ops:
  0.0 323.1 %shard_map.73 = bf16[128,2048]{1,0:T(8,128)(2,1)} custom-call(bf16[128,2048]{1,0:T(8,128)(2,1)} %tokens_hbm.1, f32[1,2048]{1,0:T(1,128)} %bitcast.3, s32[2,128]{1,0:T(2,128)} %bitcast.4, f32[2,128]{1,0:T(2,128)} %bitcast.5, bf16[1,2048,512]{2,1,0:T(8,128)(2,1)} %gate_hbm.1, bf16[1,2048,512]{2,1,0:T(8,128)(2,1)} %up_hbm.1, bf16[1,512,2048]{2,1,0:T(8,128)(2,1)} %down_hbm.1), custom_call_target="tpu_custom_call" | custom-call | tf_op jit(solution)/shard_map/pallas_call | solution.py:453
  323.1 1.9 copy.9

commit v5 on v4

--- a/solution.py
+++ b/solution.py
@@ -415,7 +415,7 @@
     tok, width = tokens.shape
     hidden = gate_weight.shape[2]
     experts, side, cap, half, radii, thin = plan(devices, tok, expert_ids.shape[1])
-    piece = cap
+    piece = cap // 2
     vmem = pl.BlockSpec(memory_space=pltpu.VMEM)
     hbm = pl.BlockSpec(memory_space=pl.ANY)
     dma = pltpu.SemaphoreType.DMA
@@ -425,7 +425,7 @@
         scratch += [
             pltpu.VMEM((2, steps, half, width), BF16),
             pltpu.VMEM((2, steps, half, width), BF16),
-            pltpu.VMEM((2, steps, 8, tok), F32),
+            pltpu.VMEM((2, steps, 4, tok), F32),
             pltpu.VMEM((SLOTS, 4 * cap, width), BF16),
             pltpu.VMEM((2, 2 * cap, width), F32),
             pltpu.VMEM((2, 2 * cap, width), BF16),

time: 325 us -> 324 us (level)
  no operation moved by 1% of the time
where the time goes in v5:
time: 324 us; the launch traced here: 323 us
  Pallas kernels  321 us (99%)
    pallas_call x1, Pallas kernels, body(): pl.pallas_call(functools.partial(kernel, devices, piece), out_shape=jax.S...  321 us

profile of v5, /device:TPU:38, one launch (start us, length us, event | category | flops | bytes accessed | tf_op | source)
XLA Modules:
  0.0 323.3 jit_solution(1472252811582464054)
XLA Ops:
  0.0 321.4 %shard_map.73 = bf16[128,2048]{1,0:T(8,128)(2,1)} custom-call(bf16[128,2048]{1,0:T(8,128)(2,1)} %tokens_hbm.1, f32[1,2048]{1,0:T(1,128)} %bitcast.3, s32[2,128]{1,0:T(2,128)} %bitcast.4, f32[2,128]{1,0:T(2,128)} %bitcast.5, bf16[1,2048,512]{2,1,0:T(8,128)(2,1)} %gate_hbm.1, bf16[1,2048,512]{2,1,0:T(8,128)(2,1)} %up_hbm.1, bf16[1,512,2048]{2,1,0:T(8,128)(2,1)} %down_hbm.1), custom_call_target="tpu_custom_call" | custom-call | tf_op jit(solution)/shard_map/pallas_call | solution.py:453
  321.4 1.9 copy.9

commit v6 on v5

--- a/solution.py
+++ b/solution.py
@@ -237,8 +237,9 @@
             fact = [sorted_facts[i : i + 1] for i in range(10)]
             meta[w][way, 0] = jnp.full(meta[w].shape[2:], -1.0, F32)
             for i in range(2):
-                meta[w][way, 0, i : i + 1, 0:half] = fact[i] * float(cap) + fact[2 + i]
-                meta[w][way, 0, 2 + i : 3 + i, 0:half] = (
+                lanes = slice(i * half, (i + 1) * half)
+                meta[w][way, 0, 0:1, lanes] = fact[i] * float(cap) + fact[2 + i]
+                meta[w][way, 0, 1:2, lanes] = (
                     fact[4 + 3 * i] + fact[5 + 3 * i] + fact[6 + 3 * i]
                 )
 
@@ -265,7 +266,8 @@
 
     def matches(w, way, k):
         slots = lax.broadcasted_iota(jnp.int32, (cap, half), 0).astype(F32) + first_code
-        return meta[w][way, k, 0:1, 0:half] == slots, meta[w][way, k, 1:2, 0:half] == slots
+        code = meta[w][way, k, 0:1, :]
+        return code[:, 0:half] == slots, code[:, half : 2 * half] == slots
 
     def onehot(w, way, k):
         first, second = matches(w, way, k)
@@ -317,9 +319,10 @@
         slot = lax.rem(k, 2)
         for way in range(2):
             first, second = matches(w, way, k)
+            share = meta[w][way, k, 1:2, :]
             scale = jnp.sum(
-                jnp.where(first, meta[w][way, k, 2:3, 0:half], 0.0)
-                + jnp.where(second, meta[w][way, k, 3:4, 0:half], 0.0),
+                jnp.where(first, share[:, 0:half], 0.0)
+                + jnp.where(second, share[:, half : 2 * half], 0.0),
                 axis=1,
                 keepdims=True,
             )
@@ -388,7 +391,7 @@
                 preferred_element_type=F32,
             )
             total = share if total is None else total + share
-    out_ref[...] = total.astype(BF16)
+    out_ref[...] = total
 
     def finish(w, way, first):
         peer = upper if way == 0 else lower
@@ -425,7 +428,7 @@
         scratch += [
             pltpu.VMEM((2, steps, half, width), BF16),
             pltpu.VMEM((2, steps, half, width), BF16),
-            pltpu.VMEM((2, steps, 4, tok), F32),
+            pltpu.VMEM((2, steps, 2, tok), F32),
             pltpu.VMEM((SLOTS, 4 * cap, width), BF16),
             pltpu.VMEM((2, 2 * cap, width), F32),
             pltpu.VMEM((2, 2 * cap, width), BF16),
@@ -452,7 +455,7 @@
     ]
     return pl.pallas_call(
         functools.partial(kernel, devices, piece),
-        out_shape=jax.ShapeDtypeStruct((tok, width), BF16),
+        out_shape=jax.ShapeDtypeStruct((tok, width), F32),
         in_specs=[hbm] + [vmem] * 3 + [hbm] * 3,
         out_specs=vmem,
         scratch_shapes=scratch,
@@ -467,7 +470,7 @@
         gate_weight,
         up_weight,
         down_weight,
-    )
+    ).astype(BF16)
 
 
 def solution(mesh):

time: 324 us -> 323 us (level)
  no operation moved by 1% of the time
where the time goes in v6:
time: 323 us
  Pallas kernels  321 us (99%)
    pallas_call x1, Pallas kernels, body(): pl.pallas_call(functools.partial(kernel, devices, piece), out_shape=jax.S...  321 us

profile of v6, /device:TPU:38, one launch (start us, length us, event | category | flops | bytes accessed | tf_op | source)
XLA Modules:
  0.0 323.2 jit_solution(7714784416692699506)
XLA Ops:
  0.0 321.1 %shard_map.73 = f32[128,2048]{1,0:T(8,128)} custom-call(bf16[128,2048]{1,0:T(8,128)(2,1)} %tokens_hbm.1, f32[1,2048]{1,0:T(1,128)} %bitcast.3, s32[2,128]{1,0:T(2,128)} %bitcast.4, f32[2,128]{1,0:T(2,128)} %bitcast.5, bf16[1,2048,512]{2,1,0:T(8,128)(2,1)} %gate_hbm.1, bf16[1,2048,512]{2,1,0:T(8,128)(2,1)} %up_hbm.1, bf16[1,512,2048]{2,1,0:T(8,128)(2,1)} %down_hbm.1), custom_call_target="tpu_custom_call" | custom-call | tf_op jit(solution)/shard_map/pallas_call | solution.py:456
  321.1 2.1 convert_element_type.3
